TPU v7x, 256 devices: a whole 4x4x8 slice. The times are simulated.
256 devices in a mesh: sp: 32 (over z, y), tp: 8 (over x, core).
Axes of the slice: x: 4, y: 4, z: 8, core: 2. Of those that a mesh axis runs over, the one named last changes fastest.
Arguments:
- activations: bfloat16 [14336, 2048], P(('sp', 'tp')), may hold values from -27.5 to 27.5
- query_weight: bfloat16 [2048, 2048], P(None, 'tp'), may hold values from -0.088388348 to 0.088388348
- key_weight: bfloat16 [2048, 2048], P(None, 'tp'), may hold values from -0.088388348 to 0.088388348
- value_weight: bfloat16 [2048, 2048], P(None, 'tp'), may hold values from -0.125 to 0.125
- out_weight: bfloat16 [2048, 2048], P('tp'), may hold values from -0.125 to 0.125
- lambdas: float32 [8], P('tp'), may hold values from 0.3 to 0.8
- head_gain: float32 [256], replicated, may hold values from 0.1 to 1.9
Outputs:
- mixed: bfloat16 [14336, 2048], P(('sp', 'tp'))
All inputs are finite; a program needn't handle non-finite values.
Results may differ from a plain program's by a relative error of at most 0.014.
Values may be sent and summed in bfloat16 or wider, within the bound.
A program may use at most 128 MiB of HBM per device.

v0:
```python
import math

import jax
import jax.numpy as jnp
from jax import lax
from jax.sharding import PartitionSpec as P

HEAD = 128
VALUE = 256


norm_floor = 0.02
very_low = -1e30


def in_order(parts, dim):
    parts = jnp.moveaxis(parts, 0, dim)
    dims = parts.shape
    return parts.reshape(*dims[:dim], dims[dim] * dims[dim + 1], *dims[dim + 2 :])


def from_everyone(array, axis):
    copies = jnp.broadcast_to(array, (lax.axis_size(axis), *array.shape))
    return lax.all_to_all(copies, axis, split_axis=0, concat_axis=0, tiled=True)


def gathered_copies(array, axis, dim):
    return in_order(from_everyone(array, axis), dim)


def in_one_piece(arrays, axis, dim, along):
    both = jnp.concatenate(arrays, axis=along)
    out, at, gathered = (lax.all_gather(both, axis, axis=dim, tiled=True), 0, [])
    for a in arrays:
        gathered.append(lax.slice_in_dim(out, at, at + a.shape[along], axis=along))
        at += a.shape[along]
    return tuple(gathered)


def in_blocks(array, dim, length):
    dims = array.shape
    parts = array.reshape(*dims[:dim], length, dims[dim] // length, *dims[dim + 1 :])
    return jnp.moveaxis(parts, dim, 0)


def sent_and_summed(array, axis, dim):
    length = lax.axis_size(axis)
    parts = lax.all_to_all(in_blocks(array, dim, length), axis, 0, 0, tiled=True)
    return jnp.sum(parts.astype(jnp.float32), axis=0)


def empty_state(count, local_heads):
    return (
        jnp.full((local_heads, 2, count), very_low, jnp.float32),
        jnp.zeros((local_heads, 2, count), jnp.float32),
        jnp.zeros((local_heads, 2, count, VALUE), jnp.float32),
    )


def absorb(state, query_set, query_pos, key_block, value_block, key_first):
    running, denoms, accums = state
    local_heads = running.shape[0]
    span = key_block.shape[0]
    key_grid = key_block.reshape(span, local_heads, 2, HEAD)
    scores = jnp.einsum(
        "qhme,khme->hmqk", query_set, key_grid, preferred_element_type=jnp.float32
    ) * HEAD ** (-0.5)
    key_pos = key_first + jnp.arange(span, dtype=jnp.int32)
    allowed = key_pos[None, :] <= query_pos[:, None]
    masked = jnp.where(allowed, scores, very_low)
    updated = jnp.maximum(running, jnp.max(masked, axis=-1))
    exp_weights = jnp.where(allowed, jnp.exp(masked - updated[..., None]), 0.0)
    factor = jnp.exp(running - updated)
    denoms = denoms * factor + jnp.sum(exp_weights, axis=-1)
    value_grid = value_block.reshape(span, local_heads, VALUE)
    product = jnp.einsum(
        "hmqk,khv->hmqv",
        exp_weights.astype(jnp.bfloat16),
        value_grid,
        preferred_element_type=jnp.float32,
    )
    accums = accums * factor[..., None] + product
    return (updated, denoms, accums)


def make_folder(query_sets, carry, pieces):
    key_piece, value_piece = pieces
    length = key_piece.shape[0]
    span = math.gcd(length, 512)

    def one_span(span_index, states):
        offset = span_index * span
        key_block = lax.dynamic_slice_in_dim(key_piece, offset, span, 0)
        value_block = lax.dynamic_slice_in_dim(value_piece, offset, span, 0)
        fresh = []
        for state, query_entry in zip(states, query_sets):
            query_set, query_pos = query_entry

            def take(current):
                return absorb(current, query_set, query_pos, key_block, value_block, offset)

            def leave(current):
                return current

            fresh.append(lax.cond(offset <= query_pos[-1], take, leave, state))
        return tuple(fresh)

    return lax.fori_loop(0, length // span, one_span, carry)


def shards(activations, query_weight, key_weight, value_weight, out_weight, lambdas, head_gain):
    local_heads = lambdas.shape[0]
    query_width = query_weight.shape[1]
    joined_weight = jnp.concatenate([query_weight, key_weight, value_weight], axis=1)
    projected = jnp.dot(
        gathered_copies(activations, "tp", 0), joined_weight, preferred_element_type=jnp.float32
    ).astype(jnp.bfloat16)
    row_count = projected.shape[0]
    queries = projected[:, :query_width].reshape(row_count, local_heads, 2, HEAD)
    key_rows = projected[:, query_width : 2 * query_width]
    value_rows = projected[:, 2 * query_width :]
    position = lax.axis_index("sp") * row_count + jnp.arange(row_count, dtype=jnp.int32)
    query_sets = [(queries, position)]
    start_states = tuple((empty_state(entry[0].shape[0], local_heads) for entry in query_sets))
    finals = make_folder(query_sets, start_states, in_one_piece((key_rows, value_rows), "sp", 0, 1))
    outputs = []
    for state in finals:
        running, denoms, accums = state
        combined = (
            accums[:, 0] / denoms[:, 0, :, None]
            - lambdas[:, None, None] * accums[:, 1] / denoms[:, 1, :, None]
        )
        inverse_rms = lax.rsqrt(jnp.mean(combined * combined, axis=-1, keepdims=True) + norm_floor)
        normed = (combined * inverse_rms * head_gain).astype(jnp.bfloat16)
        outputs.append(
            jnp.transpose(normed, (1, 0, 2)).reshape(normed.shape[1], local_heads * VALUE)
        )
    heads_out = outputs[0]
    mixed = sent_and_summed(
        jnp.dot(heads_out, out_weight, preferred_element_type=jnp.float32).astype(jnp.bfloat16),
        "tp",
        0,
    )
    return mixed.astype(jnp.bfloat16)


def solution(mesh):
    in_specs = (
        P(("sp", "tp"), None),
        P(None, "tp"),
        P(None, "tp"),
        P(None, "tp"),
        P("tp", None),
        P("tp"),
        P(),
    )
    out_specs = P(("sp", "tp"), None)
    return jax.shard_map(shards, mesh=mesh, in_specs=in_specs, out_specs=out_specs, check_vma=False)
```

profile of v0, /device:TPU:240, one launch (start us, length us, event | category | flops | bytes accessed | tf_op | source)
XLA Modules:
  0.0 385.3 jit_solution(15885949706950607097)
XLA Ops:
  7.8 28.8 %all_to_all.10 = bf16[8,56,2048]{2,1,0:T(8,128)(2,1)S(1)} all-to-all(bf16[8,56,2048]{2,1,0:T(8,128)(2,1)S(1)} %broadcast_in_dim.34), channel_id=1, replica_groups=mesh['sp'=32,'tp'=8] {'tp'}, dimensions={0} | all-to-all | bytes 3670016 | tf_op jit(solution)/shard_map/all_to_all | solution.py:24
  39.8 123.8 %all-gather.2.cloned.1.call-done = bf16[14336,512]{1,0:T(8,128)(2,1)} async-done(((bf16[448,512]{1,0:T(8,128)(2,1)}), bf16[14336,512]{1,0:T(8,128)(2,1)}) %all-gather.2.cloned.1.call-update) | async-done | bytes 14680080 | tf_op jit(solution)/shard_map/all_gather | solution.py:33
  163.7 10.3 %fusion.45 = (bf16[14336,256]{1,0:T(8,128)(2,1)}, bf16[14336,256]{1,0:T(8,128)(2,1)}) fusion(bf16[14336,512]{1,0:T(8,128)(2,1)} %all-gather.2.cloned.1.call-done), kind=kLoop, calls=%fused_computation.56 | loop fusion | bytes 29360128 | tf_op jit(solution)/shard_map/slice | solution.py:35
  174.0 10.1 %copy.10 = bf16[14336,256]{0,1:T(8,128)(2,1)} copy(bf16[14336,256]{1,0:T(8,128)(2,1)} %get-tuple-element.297) | data formatting | bytes 14680064 | tf_op jit(solution)/shard_map/while | solution.py:108
  184.2 163.6 %while.17 = (s32[]{:T(128)}, f32[1,2,448]{2,1,0:T(2,128)S(1)}, f32[1,2,448]{2,1,0:T(2,128)S(1)}, f32[1,2,448,256]{3,2,1,0:T(8,128)S(1)}, s32[448]{0:T(512)S(1)},...) while((s32[]{:T(128)}, f32[1,2,448]{2,1,0:T(2,128)S(1)}, ...), condition=%wide.region_5.6_spmd, body=%wide.region_0.5_spmd.sunk | while | flops 358976640 | bytes 9599021 | solution.py:108
  197.2 4.6 %conditional.2 = ((f32[1,2,448]{2,1,0:T(2,128)S(1)}, f32[1,2,448]{2,1,0:T(2,128)S(1)}, f32[1,2,448,256]{3,2,1,0:T(8,128)S(1)})) conditional(s32[]{:T(128)} %convert_element_type.44, (f32[1,2,448]{2,1,0:T(2,128)S(1)}, f32[1,2,448]{2,1,0:T(2,128)S(1)}, f32[1,2,448,256]{3,2,1,0:T(8,128)S(1)}) %tuple.52, (s32[]{:T(128)}, s32[448]{0:T(512)S(1)}, ...), branch_computations={%region_1.0_spmd, %region_2.4_spmd} | conditional | flops 358976640 | bytes 9598798 | solution.py:105
  203.0 4.6 %conditional.2 = ((f32[1,2,448]{2,1,0:T(2,128)S(1)}, f32[1,2,448]{2,1,0:T(2,128)S(1)}, f32[1,2,448,256]{3,2,1,0:T(8,128)S(1)})) conditional(s32[]{:T(128)} %convert_element_type.44, (f32[1,2,448]{2,1,0:T(2,128)S(1)}, f32[1,2,448]{2,1,0:T(2,128)S(1)}, f32[1,2,448,256]{3,2,1,0:T(8,128)S(1)}) %tuple.52, (s32[]{:T(128)}, s32[448]{0:T(512)S(1)}, ...), branch_computations={%region_1.0_spmd, %region_2.4_spmd} | conditional | flops 358976640 | bytes 9598798 | solution.py:105
  208.9 4.6 %conditional.2 = ((f32[1,2,448]{2,1,0:T(2,128)S(1)}, f32[1,2,448]{2,1,0:T(2,128)S(1)}, f32[1,2,448,256]{3,2,1,0:T(8,128)S(1)})) conditional(s32[]{:T(128)} %convert_element_type.44, (f32[1,2,448]{2,1,0:T(2,128)S(1)}, f32[1,2,448]{2,1,0:T(2,128)S(1)}, f32[1,2,448,256]{3,2,1,0:T(8,128)S(1)}) %tuple.52, (s32[]{:T(128)}, s32[448]{0:T(512)S(1)}, ...), branch_computations={%region_1.0_spmd, %region_2.4_spmd} | conditional | flops 358976640 | bytes 9598798 | solution.py:105
  214.7 4.6 %conditional.2 = ((f32[1,2,448]{2,1,0:T(2,128)S(1)}, f32[1,2,448]{2,1,0:T(2,128)S(1)}, f32[1,2,448,256]{3,2,1,0:T(8,128)S(1)})) conditional(s32[]{:T(128)} %convert_element_type.44, (f32[1,2,448]{2,1,0:T(2,128)S(1)}, f32[1,2,448]{2,1,0:T(2,128)S(1)}, f32[1,2,448,256]{3,2,1,0:T(8,128)S(1)}) %tuple.52, (s32[]{:T(128)}, s32[448]{0:T(512)S(1)}, ...), branch_computations={%region_1.0_spmd, %region_2.4_spmd} | conditional | flops 358976640 | bytes 9598798 | solution.py:105
  220.5 4.6 %conditional.2 = ((f32[1,2,448]{2,1,0:T(2,128)S(1)}, f32[1,2,448]{2,1,0:T(2,128)S(1)}, f32[1,2,448,256]{3,2,1,0:T(8,128)S(1)})) conditional(s32[]{:T(128)} %convert_element_type.44, (f32[1,2,448]{2,1,0:T(2,128)S(1)}, f32[1,2,448]{2,1,0:T(2,128)S(1)}, f32[1,2,448,256]{3,2,1,0:T(8,128)S(1)}) %tuple.52, (s32[]{:T(128)}, s32[448]{0:T(512)S(1)}, ...), branch_computations={%region_1.0_spmd, %region_2.4_spmd} | conditional | flops 358976640 | bytes 9598798 | solution.py:105
  226.4 4.6 %conditional.2 = ((f32[1,2,448]{2,1,0:T(2,128)S(1)}, f32[1,2,448]{2,1,0:T(2,128)S(1)}, f32[1,2,448,256]{3,2,1,0:T(8,128)S(1)})) conditional(s32[]{:T(128)} %convert_element_type.44, (f32[1,2,448]{2,1,0:T(2,128)S(1)}, f32[1,2,448]{2,1,0:T(2,128)S(1)}, f32[1,2,448,256]{3,2,1,0:T(8,128)S(1)}) %tuple.52, (s32[]{:T(128)}, s32[448]{0:T(512)S(1)}, ...), branch_computations={%region_1.0_spmd, %region_2.4_spmd} | conditional | flops 358976640 | bytes 9598798 | solution.py:105
  232.2 4.6 %conditional.2 = ((f32[1,2,448]{2,1,0:T(2,128)S(1)}, f32[1,2,448]{2,1,0:T(2,128)S(1)}, f32[1,2,448,256]{3,2,1,0:T(8,128)S(1)})) conditional(s32[]{:T(128)} %convert_element_type.44, (f32[1,2,448]{2,1,0:T(2,128)S(1)}, f32[1,2,448]{2,1,0:T(2,128)S(1)}, f32[1,2,448,256]{3,2,1,0:T(8,128)S(1)}) %tuple.52, (s32[]{:T(128)}, s32[448]{0:T(512)S(1)}, ...), branch_computations={%region_1.0_spmd, %region_2.4_spmd} | conditional | flops 358976640 | bytes 9598798 | solution.py:105
  238.1 4.6 %conditional.2 = ((f32[1,2,448]{2,1,0:T(2,128)S(1)}, f32[1,2,448]{2,1,0:T(2,128)S(1)}, f32[1,2,448,256]{3,2,1,0:T(8,128)S(1)})) conditional(s32[]{:T(128)} %convert_element_type.44, (f32[1,2,448]{2,1,0:T(2,128)S(1)}, f32[1,2,448]{2,1,0:T(2,128)S(1)}, f32[1,2,448,256]{3,2,1,0:T(8,128)S(1)}) %tuple.52, (s32[]{:T(128)}, s32[448]{0:T(512)S(1)}, ...), branch_computations={%region_1.0_spmd, %region_2.4_spmd} | conditional | flops 358976640 | bytes 9598798 | solution.py:105
  243.9 4.6 %conditional.2 = ((f32[1,2,448]{2,1,0:T(2,128)S(1)}, f32[1,2,448]{2,1,0:T(2,128)S(1)}, f32[1,2,448,256]{3,2,1,0:T(8,128)S(1)})) conditional(s32[]{:T(128)} %convert_element_type.44, (f32[1,2,448]{2,1,0:T(2,128)S(1)}, f32[1,2,448]{2,1,0:T(2,128)S(1)}, f32[1,2,448,256]{3,2,1,0:T(8,128)S(1)}) %tuple.52, (s32[]{:T(128)}, s32[448]{0:T(512)S(1)}, ...), branch_computations={%region_1.0_spmd, %region_2.4_spmd} | conditional | flops 358976640 | bytes 9598798 | solution.py:105
  249.8 4.6 %conditional.2 = ((f32[1,2,448]{2,1,0:T(2,128)S(1)}, f32[1,2,448]{2,1,0:T(2,128)S(1)}, f32[1,2,448,256]{3,2,1,0:T(8,128)S(1)})) conditional(s32[]{:T(128)} %convert_element_type.44, (f32[1,2,448]{2,1,0:T(2,128)S(1)}, f32[1,2,448]{2,1,0:T(2,128)S(1)}, f32[1,2,448,256]{3,2,1,0:T(8,128)S(1)}) %tuple.52, (s32[]{:T(128)}, s32[448]{0:T(512)S(1)}, ...), branch_computations={%region_1.0_spmd, %region_2.4_spmd} | conditional | flops 358976640 | bytes 9598798 | solution.py:105
  255.6 4.6 %conditional.2 = ((f32[1,2,448]{2,1,0:T(2,128)S(1)}, f32[1,2,448]{2,1,0:T(2,128)S(1)}, f32[1,2,448,256]{3,2,1,0:T(8,128)S(1)})) conditional(s32[]{:T(128)} %convert_element_type.44, (f32[1,2,448]{2,1,0:T(2,128)S(1)}, f32[1,2,448]{2,1,0:T(2,128)S(1)}, f32[1,2,448,256]{3,2,1,0:T(8,128)S(1)}) %tuple.52, (s32[]{:T(128)}, s32[448]{0:T(512)S(1)}, ...), branch_computations={%region_1.0_spmd, %region_2.4_spmd} | conditional | flops 358976640 | bytes 9598798 | solution.py:105
  261.5 4.6 %conditional.2 = ((f32[1,2,448]{2,1,0:T(2,128)S(1)}, f32[1,2,448]{2,1,0:T(2,128)S(1)}, f32[1,2,448,256]{3,2,1,0:T(8,128)S(1)})) conditional(s32[]{:T(128)} %convert_element_type.44, (f32[1,2,448]{2,1,0:T(2,128)S(1)}, f32[1,2,448]{2,1,0:T(2,128)S(1)}, f32[1,2,448,256]{3,2,1,0:T(8,128)S(1)}) %tuple.52, (s32[]{:T(128)}, s32[448]{0:T(512)S(1)}, ...), branch_computations={%region_1.0_spmd, %region_2.4_spmd} | conditional | flops 358976640 | bytes 9598798 | solution.py:105
  267.3 4.6 %conditional.2 = ((f32[1,2,448]{2,1,0:T(2,128)S(1)}, f32[1,2,448]{2,1,0:T(2,128)S(1)}, f32[1,2,448,256]{3,2,1,0:T(8,128)S(1)})) conditional(s32[]{:T(128)} %convert_element_type.44, (f32[1,2,448]{2,1,0:T(2,128)S(1)}, f32[1,2,448]{2,1,0:T(2,128)S(1)}, f32[1,2,448,256]{3,2,1,0:T(8,128)S(1)}) %tuple.52, (s32[]{:T(128)}, s32[448]{0:T(512)S(1)}, ...), branch_computations={%region_1.0_spmd, %region_2.4_spmd} | conditional | flops 358976640 | bytes 9598798 | solution.py:105
  273.1 4.6 %conditional.2 = ((f32[1,2,448]{2,1,0:T(2,128)S(1)}, f32[1,2,448]{2,1,0:T(2,128)S(1)}, f32[1,2,448,256]{3,2,1,0:T(8,128)S(1)})) conditional(s32[]{:T(128)} %convert_element_type.44, (f32[1,2,448]{2,1,0:T(2,128)S(1)}, f32[1,2,448]{2,1,0:T(2,128)S(1)}, f32[1,2,448,256]{3,2,1,0:T(8,128)S(1)}) %tuple.52, (s32[]{:T(128)}, s32[448]{0:T(512)S(1)}, ...), branch_computations={%region_1.0_spmd, %region_2.4_spmd} | conditional | flops 358976640 | bytes 9598798 | solution.py:105
  279.0 4.6 %conditional.2 = ((f32[1,2,448]{2,1,0:T(2,128)S(1)}, f32[1,2,448]{2,1,0:T(2,128)S(1)}, f32[1,2,448,256]{3,2,1,0:T(8,128)S(1)})) conditional(s32[]{:T(128)} %convert_element_type.44, (f32[1,2,448]{2,1,0:T(2,128)S(1)}, f32[1,2,448]{2,1,0:T(2,128)S(1)}, f32[1,2,448,256]{3,2,1,0:T(8,128)S(1)}) %tuple.52, (s32[]{:T(128)}, s32[448]{0:T(512)S(1)}, ...), branch_computations={%region_1.0_spmd, %region_2.4_spmd} | conditional | flops 358976640 | bytes 9598798 | solution.py:105
  284.8 4.6 %conditional.2 = ((f32[1,2,448]{2,1,0:T(2,128)S(1)}, f32[1,2,448]{2,1,0:T(2,128)S(1)}, f32[1,2,448,256]{3,2,1,0:T(8,128)S(1)})) conditional(s32[]{:T(128)} %convert_element_type.44, (f32[1,2,448]{2,1,0:T(2,128)S(1)}, f32[1,2,448]{2,1,0:T(2,128)S(1)}, f32[1,2,448,256]{3,2,1,0:T(8,128)S(1)}) %tuple.52, (s32[]{:T(128)}, s32[448]{0:T(512)S(1)}, ...), branch_computations={%region_1.0_spmd, %region_2.4_spmd} | conditional | flops 358976640 | bytes 9598798 | solution.py:105
  290.7 4.6 %conditional.2 = ((f32[1,2,448]{2,1,0:T(2,128)S(1)}, f32[1,2,448]{2,1,0:T(2,128)S(1)}, f32[1,2,448,256]{3,2,1,0:T(8,128)S(1)})) conditional(s32[]{:T(128)} %convert_element_type.44, (f32[1,2,448]{2,1,0:T(2,128)S(1)}, f32[1,2,448]{2,1,0:T(2,128)S(1)}, f32[1,2,448,256]{3,2,1,0:T(8,128)S(1)}) %tuple.52, (s32[]{:T(128)}, s32[448]{0:T(512)S(1)}, ...), branch_computations={%region_1.0_spmd, %region_2.4_spmd} | conditional | flops 358976640 | bytes 9598798 | solution.py:105
  296.5 4.6 %conditional.2 = ((f32[1,2,448]{2,1,0:T(2,128)S(1)}, f32[1,2,448]{2,1,0:T(2,128)S(1)}, f32[1,2,448,256]{3,2,1,0:T(8,128)S(1)})) conditional(s32[]{:T(128)} %convert_element_type.44, (f32[1,2,448]{2,1,0:T(2,128)S(1)}, f32[1,2,448]{2,1,0:T(2,128)S(1)}, f32[1,2,448,256]{3,2,1,0:T(8,128)S(1)}) %tuple.52, (s32[]{:T(128)}, s32[448]{0:T(512)S(1)}, ...), branch_computations={%region_1.0_spmd, %region_2.4_spmd} | conditional | flops 358976640 | bytes 9598798 | solution.py:105
  302.4 4.6 %conditional.2 = ((f32[1,2,448]{2,1,0:T(2,128)S(1)}, f32[1,2,448]{2,1,0:T(2,128)S(1)}, f32[1,2,448,256]{3,2,1,0:T(8,128)S(1)})) conditional(s32[]{:T(128)} %convert_element_type.44, (f32[1,2,448]{2,1,0:T(2,128)S(1)}, f32[1,2,448]{2,1,0:T(2,128)S(1)}, f32[1,2,448,256]{3,2,1,0:T(8,128)S(1)}) %tuple.52, (s32[]{:T(128)}, s32[448]{0:T(512)S(1)}, ...), branch_computations={%region_1.0_spmd, %region_2.4_spmd} | conditional | flops 358976640 | bytes 9598798 | solution.py:105
  308.2 4.6 %conditional.2 = ((f32[1,2,448]{2,1,0:T(2,128)S(1)}, f32[1,2,448]{2,1,0:T(2,128)S(1)}, f32[1,2,448,256]{3,2,1,0:T(8,128)S(1)})) conditional(s32[]{:T(128)} %convert_element_type.44, (f32[1,2,448]{2,1,0:T(2,128)S(1)}, f32[1,2,448]{2,1,0:T(2,128)S(1)}, f32[1,2,448,256]{3,2,1,0:T(8,128)S(1)}) %tuple.52, (s32[]{:T(128)}, s32[448]{0:T(512)S(1)}, ...), branch_computations={%region_1.0_spmd, %region_2.4_spmd} | conditional | flops 358976640 | bytes 9598798 | solution.py:105
  314.1 4.6 %conditional.2 = ((f32[1,2,448]{2,1,0:T(2,128)S(1)}, f32[1,2,448]{2,1,0:T(2,128)S(1)}, f32[1,2,448,256]{3,2,1,0:T(8,128)S(1)})) conditional(s32[]{:T(128)} %convert_element_type.44, (f32[1,2,448]{2,1,0:T(2,128)S(1)}, f32[1,2,448]{2,1,0:T(2,128)S(1)}, f32[1,2,448,256]{3,2,1,0:T(8,128)S(1)}) %tuple.52, (s32[]{:T(128)}, s32[448]{0:T(512)S(1)}, ...), branch_computations={%region_1.0_spmd, %region_2.4_spmd} | conditional | flops 358976640 | bytes 9598798 | solution.py:105
  319.9 4.6 %conditional.2 = ((f32[1,2,448]{2,1,0:T(2,128)S(1)}, f32[1,2,448]{2,1,0:T(2,128)S(1)}, f32[1,2,448,256]{3,2,1,0:T(8,128)S(1)})) conditional(s32[]{:T(128)} %convert_element_type.44, (f32[1,2,448]{2,1,0:T(2,128)S(1)}, f32[1,2,448]{2,1,0:T(2,128)S(1)}, f32[1,2,448,256]{3,2,1,0:T(8,128)S(1)}) %tuple.52, (s32[]{:T(128)}, s32[448]{0:T(512)S(1)}, ...), branch_computations={%region_1.0_spmd, %region_2.4_spmd} | conditional | flops 358976640 | bytes 9598798 | solution.py:105
  325.7 4.6 %conditional.2 = ((f32[1,2,448]{2,1,0:T(2,128)S(1)}, f32[1,2,448]{2,1,0:T(2,128)S(1)}, f32[1,2,448,256]{3,2,1,0:T(8,128)S(1)})) conditional(s32[]{:T(128)} %convert_element_type.44, (f32[1,2,448]{2,1,0:T(2,128)S(1)}, f32[1,2,448]{2,1,0:T(2,128)S(1)}, f32[1,2,448,256]{3,2,1,0:T(8,128)S(1)}) %tuple.52, (s32[]{:T(128)}, s32[448]{0:T(512)S(1)}, ...), branch_computations={%region_1.0_spmd, %region_2.4_spmd} | conditional | flops 358976640 | bytes 9598798 | solution.py:105
  331.6 4.6 %conditional.2 = ((f32[1,2,448]{2,1,0:T(2,128)S(1)}, f32[1,2,448]{2,1,0:T(2,128)S(1)}, f32[1,2,448,256]{3,2,1,0:T(8,128)S(1)})) conditional(s32[]{:T(128)} %convert_element_type.44, (f32[1,2,448]{2,1,0:T(2,128)S(1)}, f32[1,2,448]{2,1,0:T(2,128)S(1)}, f32[1,2,448,256]{3,2,1,0:T(8,128)S(1)}) %tuple.52, (s32[]{:T(128)}, s32[448]{0:T(512)S(1)}, ...), branch_computations={%region_1.0_spmd, %region_2.4_spmd} | conditional | flops 358976640 | bytes 9598798 | solution.py:105
  337.4 4.6 %conditional.2 = ((f32[1,2,448]{2,1,0:T(2,128)S(1)}, f32[1,2,448]{2,1,0:T(2,128)S(1)}, f32[1,2,448,256]{3,2,1,0:T(8,128)S(1)})) conditional(s32[]{:T(128)} %convert_element_type.44, (f32[1,2,448]{2,1,0:T(2,128)S(1)}, f32[1,2,448]{2,1,0:T(2,128)S(1)}, f32[1,2,448,256]{3,2,1,0:T(8,128)S(1)}) %tuple.52, (s32[]{:T(128)}, s32[448]{0:T(512)S(1)}, ...), branch_computations={%region_1.0_spmd, %region_2.4_spmd} | conditional | flops 358976640 | bytes 9598798 | solution.py:105
  343.3 4.6 %conditional.2 = ((f32[1,2,448]{2,1,0:T(2,128)S(1)}, f32[1,2,448]{2,1,0:T(2,128)S(1)}, f32[1,2,448,256]{3,2,1,0:T(8,128)S(1)})) conditional(s32[]{:T(128)} %convert_element_type.44, (f32[1,2,448]{2,1,0:T(2,128)S(1)}, f32[1,2,448]{2,1,0:T(2,128)S(1)}, f32[1,2,448,256]{3,2,1,0:T(8,128)S(1)}) %tuple.52, (s32[]{:T(128)}, s32[448]{0:T(512)S(1)}, ...), branch_computations={%region_1.0_spmd, %region_2.4_spmd} | conditional | flops 358976640 | bytes 9598798 | solution.py:105
  349.0 28.5 %all_to_all.11 = bf16[8,56,2048]{2,1,0:T(8,128)(2,1)S(1)} all-to-all(bf16[8,56,2048]{2,1,0:T(8,128)(2,1)S(1)} %bitcast.80), channel_id=1, replica_groups=mesh['sp'=32,'tp'=8] {'tp'}, dimensions={0} | all-to-all | bytes 3670016 | tf_op jit(solution)/shard_map/all_to_all | solution.py:48
  (309 shorter events, 158.7 us)
Async XLA Ops:
  6.5 341.7 %copy-start = (bf16[256,2048]{1,0:T(8,128)(2,1)S(1)}, bf16[256,2048]{1,0:T(8,128)(2,1)}, u32[]{:S(2)}) copy-start(bf16[256,2048]{1,0:T(8,128)(2,1)} %param.15) | copy-start | bytes 3145732
  6.5 157.1 %all-gather.2.cloned.1.call-start = ((), (), s32[]{:S(2)}) async-start(), calls=%async_computation.2 | async-start | bytes 15138816 | tf_op jit(solution)/shard_map/all_gather | solution.py:33
  7.8 28.8 %copy-start.1 = (bf16[2048,256]{1,0:T(8,128)(2,1)S(1)}, bf16[2048,256]{1,0:T(8,128)(2,1)}, u32[]{:S(2)}) copy-start(bf16[2048,256]{1,0:T(8,128)(2,1)} %param.14) | copy-start | bytes 3145732
  7.8 28.8 %copy-start.2 = (bf16[2048,256]{1,0:T(8,128)(2,1)S(1)}, bf16[2048,256]{1,0:T(8,128)(2,1)}, u32[]{:S(2)}) copy-start(bf16[2048,256]{1,0:T(8,128)(2,1)} %param.13) | copy-start | bytes 3145732
  7.8 28.8 %copy-start.3 = (bf16[2048,256]{1,0:T(8,128)(2,1)S(1)}, bf16[2048,256]{1,0:T(8,128)(2,1)}, u32[]{:S(2)}) copy-start(bf16[2048,256]{1,0:T(8,128)(2,1)} %param.12) | copy-start | bytes 3145732
  184.2 164.0 %copy-start.4 = (f32[256]{0:T(256)S(1)}, f32[256]{0:T(256)}, u32[]{:S(2)}) copy-start(f32[256]{0:T(256)} %param.17) | copy-start | bytes 3076
Sparse Core Ops, SparseCore 0:
  39.2 124.4 all-gather.1
where the time goes:
time: 388 us; the launch traced here: 385 us
  waiting for transfers between devices  124 us (32%)
  matrix products  73.1 us (19%)
  local copies, waits for them, and re-layouts  66.6 us (17%)
  blocking collectives  57.2 us (15%)
  other arithmetic  30.3 us (8%)
  loops' own time  20.1 us (5%)
  between operations  14.2 us (4%)
    all_gather x1, waiting for transfers between devices, in_one_piece(): lax.all_gather(both, axis, axis=dim, tiled=True)  124 us
    dot_general x28, matrix products, absorb(): jnp.einsum('hmqk,khv->hmqv', exp_weights.astype(jnp.bfloat16), value_grid...  54.7 us
    all_to_all x1, blocking collectives, from_everyone(): return lax.all_to_all(copies, axis, split_axis=0, concat_axis=0, tiled=True)  28.8 us
    all_to_all x1, blocking collectives, sent_and_summed(): lax.all_to_all(in_blocks(array, dim, length), axis, 0, 0, tiled=True)  28.5 us
    dynamic_slice x28, local copies, waits for them, and re-layouts, one_span(): key_block = lax.dynamic_slice_in_dim(key_piece, offset, span, 0)  27.2 us
    reduce_sum x28, other arithmetic, absorb(): denoms = denoms * factor + jnp.sum(exp_weights, axis=-1)  22.5 us
    another operation x1, loops' own time, make_folder(): return lax.fori_loop(0, length // span, one_span, carry)  18.4 us
    slice x28, local copies, waits for them, and re-layouts, one_span(): fresh.append(lax.cond(offset <= query_pos[-1], take, leave, state))  16.6 us
  transfers between devices with their start and end apart: 1, of which 1 were waited for; matrix products, arithmetic and copies ran while one was open for 0% of the time, Pallas kernels for 0%

commit v1 on v0

v1 whole, which is shorter than its diff:
```python
import functools
import math

import jax
import jax.numpy as jnp
from jax import lax
from jax.experimental import pallas as pl
from jax.experimental.pallas import tpu as pltpu
from jax.sharding import PartitionSpec as P

HEAD = 128
VALUE = 256
norm_floor = 0.02
very_low = -1e30
EXP_SCALE = HEAD ** (-0.5) * math.log2(math.e)
MESH = pl.DeviceIdType.MESH
F32 = jnp.float32
BF16 = jnp.bfloat16


def fused(X, Y, Z, TOK, D, R, QT, *refs):
    (
        x_hbm, wq_hbm, wk_hbm, wv_hbm, wo_hbm, lam_ref, gain_ref, out_ref,
        xg, wq, wk, wv, wo, proj, kv, qg, vt, acc, stats, part,
        y_relay, y_in, y_sum, hn, d_out, d_in, sx, x_relay, x_in, x_sum,
        load_sem, xa_send, xa_recv, dd_send, dd_recv, q_send, q_recv,
        zr_send, zr_recv, zl_send, zl_recv, st_send, st_recv,
        yr_send, yr_recv, do_send, do_recv, xr_send, xr_recv,
    ) = refs
    NT = Y * TOK // QT
    half = TOK // 2
    cols = D // 2
    reach = Z // 2

    sp = lax.axis_index("sp")
    tp = lax.axis_index("tp")
    z, y = sp // Y, lax.rem(sp, Y)
    x, c = tp // 2, lax.rem(tp, 2)
    x_up, x_down, x_far = lax.rem(x + 1, X), lax.rem(x + X - 1, X), lax.rem(x + X // 2, X)
    y_up, y_down, y_far = lax.rem(y + 1, Y), lax.rem(y + Y - 1, Y), lax.rem(y + Y // 2, Y)
    z_up, z_down = lax.rem(z + 1, Z), lax.rem(z + Z - 1, Z)
    other = 1 - c

    def at_x(xx, cc):
        return (sp, xx * 2 + cc)

    def at_y(yy):
        return (z * Y + yy, tp)

    def at_z(zz):
        return (zz * Y + y, tp)

    def remote(src, dst, send, recv, where):
        return pltpu.make_async_remote_copy(
            src_ref=src, dst_ref=dst, send_sem=send, recv_sem=recv, device_id=where, device_id_type=MESH
        )

    loads = [
        pltpu.make_async_copy(a, b, load_sem.at[i])
        for i, (a, b) in enumerate(
            ((x_hbm, xg.at[tp]), (wq_hbm, wq), (wk_hbm, wk), (wv_hbm, wv), (wo_hbm, wo))
        )
    ]
    for load in loads:
        load.start()

    peers = [at_x(x, other)]
    if X > 1:
        peers += [at_x(x_up, c), at_x(x_down, c)]
    if Y > 1:
        peers += [at_y(y_up), at_y(y_down), at_y(y_far)]
    if Z > 1:
        peers += [at_z(z_up), at_z(z_down)]
    barrier = pltpu.get_barrier_semaphore()
    for peer in peers:
        pl.semaphore_signal(barrier, inc=1, device_id=peer, device_id_type=MESH)
    pl.semaphore_wait(barrier, len(peers))

    def slot(xx, cc):
        return xx * 2 + cc

    def block_copy(index, send, recv, where):
        return remote(xg.at[index], xg.at[index], send, recv, where)

    loads[0].wait()
    xa = []
    if X > 1:
        xa = [
            block_copy(tp, xa_send.at[0], xa_recv.at[0], at_x(x_up, c)),
            block_copy(tp, xa_send.at[1], xa_recv.at[1], at_x(x_down, c)),
            block_copy(
                jnp.where(c == 0, slot(x_down, c), slot(x_up, c)),
                xa_send.at[2], xa_recv.at[2], at_x(jnp.where(c == 0, x_up, x_down), c),
            ),
        ]
    dd = [block_copy(tp, dd_send.at[0], dd_recv.at[0], at_x(x, other))]
    if X > 1:
        dd += [
            block_copy(slot(x_down, c), dd_send.at[1], dd_recv.at[1], at_x(x, other)),
            block_copy(slot(x_up, c), dd_send.at[2], dd_recv.at[2], at_x(x, other)),
            block_copy(slot(x_far, c), dd_send.at[3], dd_recv.at[3], at_x(x, other)),
        ]
    if X > 1:
        xa[0].start()
        xa[1].start()
    dd[0].start()
    for load in loads[1:4]:
        load.wait()

    def project(i, carry):
        if X > 1:

            @pl.when(i == 1)
            def _():
                dd[0].wait_recv()

            @pl.when(i == 2)
            def _():
                xa[0].wait_recv()
                xa[1].wait_recv()
                xa[2].start()
                dd[1].start()
                dd[2].start()

            @pl.when(i == 4)
            def _():
                dd[1].wait_recv()
                dd[2].wait_recv()

            @pl.when(i == 6)
            def _():
                xa[2].wait_recv()
                dd[3].start()

            @pl.when(i == 7)
            def _():
                dd[3].wait_recv()

            xx = jnp.where(i < 2, x, jnp.where(i >= 6, x_far, jnp.where(lax.rem(i, 2) == 0, x_down, x_up)))
            cc = jnp.where((i == 1) | (i == 4) | (i == 5) | (i == 7), other, c)
        else:

            @pl.when(i == 1)
            def _():
                dd[0].wait_recv()

            xx = x
            cc = jnp.where(i == 1, other, c)
        index = slot(xx, cc)
        rows = pl.ds(pl.multiple_of(index * R, 8), R)
        block = xg[index]
        for n, w in enumerate((wq, wk, wv)):
            proj[rows, n * 256 : (n + 1) * 256] = jnp.dot(block, w[...], preferred_element_type=F32)
        return carry

    lax.fori_loop(0, 2 * X, project, 0)
    kv[z] = proj[:, 256:768].astype(BF16)
    q_row = pl.multiple_of(y * TOK, 16)
    qg[pl.ds(q_row, TOK), :] = proj[:, 0:256].astype(BF16)

    def z_copy(right, s, k, origin):
        rows = pl.ds(pl.multiple_of(k * half, 16), half)
        piece = kv.at[origin, rows, :]
        if right:
            return remote(piece, piece, zr_send.at[s, k], zr_recv.at[s, k], at_z(z_up))
        return remote(piece, piece, zl_send.at[s, k], zl_recv.at[s, k], at_z(z_down))

    def right_origin(zz, s):
        return lax.rem(zz - s + Z, Z)

    def left_origin(zz, s):
        return lax.rem(zz + s, Z)

    def right_goes(zz, s, k):
        return (zz - s >= 0) & (zz + 1 < Z) & ((s < reach - 1) | ((s == reach - 1) & (k == 0)))

    def left_goes(zz, s, k):
        o = left_origin(zz, s)
        return (o < reach) & ((o < reach - 1) | (k == 1)) & ((s < reach - 1) | ((s == reach - 1) & (k == 1)))

    if Z > 1:
        for k in range(2):

            @pl.when(right_goes(z, 0, k))
            def _():
                z_copy(True, 0, k, z).start()

            @pl.when(left_goes(z, 0, k))
            def _():
                z_copy(False, 0, k, z).start()

    def q_copy(yy, part_no, n, where):
        piece = qg.at[pl.ds(pl.multiple_of(yy * TOK + part_no * half, 16), half), :]
        return remote(piece, piece, q_send.at[n], q_recv.at[n], where)

    if Y > 1:
        qc = [
            q_copy(y, 0, 0, at_y(y_up)),
            q_copy(y, 1, 1, at_y(y_up)),
            q_copy(y_down, 0, 2, at_y(y_up)),
            q_copy(y, 1, 3, at_y(y_down)),
            q_copy(y, 0, 4, at_y(y_down)),
            q_copy(y_up, 1, 5, at_y(y_down)),
        ]
        for n in (0, 3, 1, 4):
            qc[n].start()
        qc[0].wait_recv()
        qc[2].start()
        qc[3].wait_recv()
        qc[5].start()
        for n in (1, 4, 2, 5):
            qc[n].wait_recv()

    vt[:, 0:TOK] = jnp.transpose(kv[z, :, 256:512].astype(F32)).astype(BF16)

    def own_tile(t, carry):
        rows = pl.ds(pl.multiple_of(t * QT, 16), QT)
        key_pos = lax.broadcasted_iota(jnp.int32, (TOK, QT), 0) + y * TOK
        query_pos = lax.broadcasted_iota(jnp.int32, (TOK, QT), 1) + t * QT
        allowed = key_pos <= query_pos
        for m in range(2):
            lanes = slice(m * HEAD, (m + 1) * HEAD)
            s = lax.dot_general(
                kv[z, :, lanes], qg[rows, lanes], (((1,), (1,)), ((), ())), preferred_element_type=F32
            )
            s = jnp.where(allowed, s, very_low)
            top = jnp.maximum(jnp.max(s, axis=0, keepdims=True), very_low)
            p = jnp.where(allowed, jnp.exp2((s - top) * EXP_SCALE), 0.0)
            stats[t, m : m + 1, :] = top
            stats[t, 2 + m : 3 + m, :] = jnp.sum(p, axis=0, keepdims=True)
            acc[t, m] = jnp.dot(vt[:, 0:TOK], p.astype(BF16), preferred_element_type=F32)
        return carry

    lax.fori_loop(0, NT, own_tile, 0)

    def attend(origin, k):
        key_rows = pl.ds(pl.multiple_of(k * half, 16), half)
        vt[:, 0:half] = jnp.transpose(kv[origin, key_rows, 256:512].astype(F32)).astype(BF16)

        def tile(t, carry):
            rows = pl.ds(pl.multiple_of(t * QT, 16), QT)
            for m in range(2):
                lanes = slice(m * HEAD, (m + 1) * HEAD)
                s = lax.dot_general(
                    kv[origin, key_rows, lanes],
                    qg[rows, lanes],
                    (((1,), (1,)), ((), ())),
                    preferred_element_type=F32,
                )
                before = stats[t, m : m + 1, :]
                top = jnp.maximum(before, jnp.max(s, axis=0, keepdims=True))
                p = jnp.exp2((s - top) * EXP_SCALE)
                factor = jnp.exp2((before - top) * EXP_SCALE)
                stats[t, m : m + 1, :] = top
                stats[t, 2 + m : 3 + m, :] = stats[t, 2 + m : 3 + m, :] * factor + jnp.sum(
                    p, axis=0, keepdims=True
                )
                acc[t, m] = acc[t, m] * factor + jnp.dot(
                    vt[:, 0:half], p.astype(BF16), preferred_element_type=F32
                )
            return carry

        lax.fori_loop(0, NT, tile, 0)

    if Z > 1:

        def event(e, carry):
            s, k = e // 2, lax.rem(e, 2)
            from_left = (z >= 1) & right_goes(z - 1, s, k)
            from_right = left_goes(z_up, s, k)
            o_left = right_origin(z_down, s)
            o_right = left_origin(z_up, s)

            @pl.when(from_left)
            def _():
                z_copy(True, s, k, o_left).wait_recv()

            @pl.when(from_left & right_goes(z, s + 1, k))
            def _():
                z_copy(True, s + 1, k, o_left).start()

            @pl.when(from_right)
            def _():
                z_copy(False, s, k, o_right).wait_recv()

            @pl.when(from_right & left_goes(z, s + 1, k))
            def _():
                z_copy(False, s + 1, k, o_right).start()

            def side(i, carry2):
                o = jnp.where(i == 0, o_left, o_right)
                use = jnp.where(i == 0, from_left, from_right & (o_right < z))

                @pl.when(use)
                def _():
                    attend(o, k)

                return carry2

            lax.fori_loop(0, 2, side, 0)
            return carry

        lax.fori_loop(0, 2 * reach, event, 0)

    if Y > 1:
        sc = [
            remote(stats.at[pl.ds(0, NT)], stats.at[pl.ds((n + 1) * NT, NT)], st_send.at[n], st_recv.at[n], at_y(yy))
            for n, yy in enumerate((y_up, y_down, y_far))
        ]
        for copy in sc:
            copy.start()
        for copy in sc:
            copy.wait_recv()

    lam = lam_ref[0]

    def combine(t, carry):
        rows = pl.ds(pl.multiple_of(t * QT, 16), QT)
        shares = []
        for m in range(2):
            own_top = stats[t, m : m + 1, :]
            tops = [own_top]
            sums = [stats[t, 2 + m : 3 + m, :]]
            if Y > 1:
                for n in range(3):
                    tops.append(stats[(n + 1) * NT + t, m : m + 1, :])
                    sums.append(stats[(n + 1) * NT + t, 2 + m : 3 + m, :])
            top = functools.reduce(jnp.maximum, tops)
            total = functools.reduce(
                jnp.add, [s * jnp.exp2((a - top) * EXP_SCALE) for a, s in zip(tops, sums)]
            )
            shares.append(jnp.exp2((own_top - top) * EXP_SCALE) / total)
        joined = acc[t, 0] * shares[0] - acc[t, 1] * (shares[1] * lam)
        part[rows, :] = jnp.transpose(joined).astype(BF16)
        return carry

    lax.fori_loop(0, NT, combine, 0)

    def owned(yy, h):
        return pl.ds(pl.multiple_of(yy * TOK + h * half, 16), half)

    low, high = pl.ds(0, half), pl.ds(half, half)
    if Y > 1:
        yr = [
            remote(part.at[owned(y_far, 0), :], y_relay.at[0], yr_send.at[0], yr_recv.at[0], at_y(y_up)),
            remote(part.at[owned(y_far, 1), :], y_relay.at[1], yr_send.at[1], yr_recv.at[1], at_y(y_down)),
            remote(part.at[owned(y_up, 1), :], y_in.at[0, high, :], yr_send.at[2], yr_recv.at[2], at_y(y_up)),
            remote(part.at[owned(y_down, 0), :], y_in.at[1, low, :], yr_send.at[3], yr_recv.at[3], at_y(y_down)),
            remote(y_sum.at[0], y_in.at[0, low, :], yr_send.at[4], yr_recv.at[4], at_y(y_up)),
            remote(y_sum.at[1], y_in.at[1, high, :], yr_send.at[5], yr_recv.at[5], at_y(y_down)),
        ]
        for n in range(4):
            yr[n].start()
        yr[0].wait_recv()
        y_sum[0] = (part[owned(y_up, 0), :].astype(F32) + y_relay[0].astype(F32)).astype(BF16)
        yr[4].start()
        yr[1].wait_recv()
        y_sum[1] = (part[owned(y_down, 1), :].astype(F32) + y_relay[1].astype(F32)).astype(BF16)
        yr[5].start()
        for n in range(2, 6):
            yr[n].wait_recv()
    combined = part[pl.ds(q_row, TOK), :].astype(F32)
    if Y > 1:
        combined = combined + y_in[0].astype(F32) + y_in[1].astype(F32)
    inverse_rms = lax.rsqrt(jnp.mean(combined * combined, axis=-1, keepdims=True) + norm_floor)
    hn[...] = combined * inverse_rms * gain_ref[...]

    loads[4].wait()

    def owner(j):
        if X == 1:
            return x
        return jnp.where(j == 0, x_far, jnp.where(j == 1, x_up, jnp.where(j == 2, x_down, x)))

    def shared(j, cc):
        index = slot(owner(j), cc)
        rows = pl.ds(pl.multiple_of(index * R, 8), R)
        return jnp.dot(hn[rows, :].astype(BF16), wo[...], preferred_element_type=F32)

    def d_copy(j):
        return remote(d_out.at[j], d_in.at[j], do_send.at[j], do_recv.at[j], at_x(x, other))

    def for_other(j, carry):
        d_out[j] = shared(j, other).astype(BF16)
        d_copy(j).start()
        return carry

    lax.fori_loop(0, X, for_other, 0)
    left, right = pl.ds(0, cols), pl.ds(cols, cols)
    if X > 1:
        xr = [
            remote(sx.at[0, :, left], x_relay.at[0], xr_send.at[0], xr_recv.at[0], at_x(x_up, c)),
            remote(sx.at[0, :, right], x_relay.at[1], xr_send.at[1], xr_recv.at[1], at_x(x_down, c)),
            remote(sx.at[1, :, right], x_in.at[0, :, right], xr_send.at[2], xr_recv.at[2], at_x(x_up, c)),
            remote(sx.at[2, :, left], x_in.at[1, :, left], xr_send.at[3], xr_recv.at[3], at_x(x_down, c)),
            remote(x_sum.at[0], x_in.at[0, :, left], xr_send.at[4], xr_recv.at[4], at_x(x_up, c)),
            remote(x_sum.at[1], x_in.at[1, :, right], xr_send.at[5], xr_recv.at[5], at_x(x_down, c)),
        ]

    def for_own(j, carry):
        mine = shared(j, c)
        d_copy(j).wait_recv()
        sx[j] = (mine + d_in[j].astype(F32)).astype(BF16)
        if X > 1:

            @pl.when(j == 0)
            def _():
                xr[0].start()
                xr[1].start()

            @pl.when(j == 1)
            def _():
                xr[2].start()

            @pl.when(j == 2)
            def _():
                xr[3].start()

        return carry

    lax.fori_loop(0, X, for_own, 0)
    if X > 1:
        xr[0].wait_recv()
        x_sum[0] = (sx[1, :, 0:cols].astype(F32) + x_relay[0].astype(F32)).astype(BF16)
        xr[4].start()
        xr[1].wait_recv()
        x_sum[1] = (sx[2, :, cols : 2 * cols].astype(F32) + x_relay[1].astype(F32)).astype(BF16)
        xr[5].start()
        for n in range(2, 6):
            xr[n].wait_recv()
        out_ref[...] = (
            sx[3].astype(F32) + x_in[0].astype(F32) + x_in[1].astype(F32)
        ).astype(BF16)
    else:
        out_ref[...] = sx[0]

    if X > 1:
        for copy in xa + xr:
            copy.wait_send()
    for copy in dd:
        copy.wait_send()
    for j in range(X):
        d_copy(j).wait_send()
    if Y > 1:
        for copy in qc + sc + yr:
            copy.wait_send()
    if Z > 1:

        def drain(e, carry):
            s, k = e // 2, lax.rem(e, 2)

            @pl.when(right_goes(z, s, k))
            def _():
                z_copy(True, s, k, right_origin(z, s)).wait_send()

            @pl.when(left_goes(z, s, k))
            def _():
                z_copy(False, s, k, left_origin(z, s)).wait_send()

            return carry

        lax.fori_loop(0, 2 * reach, drain, 0)


def layer(X, Y, Z, activations, query_weight, key_weight, value_weight, out_weight, lambdas, head_gain):
    R, D = activations.shape
    TOK = R * 2 * X
    QT = 256 if (Y * TOK) % 256 == 0 else TOK
    NT = Y * TOK // QT
    half = TOK // 2
    any_space = pl.BlockSpec(memory_space=pl.ANY)
    dma = pltpu.SemaphoreType.DMA
    reach = max(Z // 2, 1)
    return pl.pallas_call(
        functools.partial(fused, X, Y, Z, TOK, D, R, QT),
        out_shape=jax.ShapeDtypeStruct((R, D), BF16),
        in_specs=[any_space] * 5
        + [pl.BlockSpec(memory_space=pltpu.SMEM), pl.BlockSpec(memory_space=pltpu.VMEM)],
        out_specs=pl.BlockSpec(memory_space=pltpu.VMEM),
        scratch_shapes=[
            pltpu.VMEM((2 * X, R, D), BF16),
            pltpu.VMEM((D, 256), BF16),
            pltpu.VMEM((D, 256), BF16),
            pltpu.VMEM((D, 256), BF16),
            pltpu.VMEM((VALUE, D), BF16),
            pltpu.VMEM((TOK, 768), F32),
            pltpu.VMEM((Z, TOK, 512), BF16),
            pltpu.VMEM((Y * TOK, 256), BF16),
            pltpu.VMEM((VALUE, 512), BF16),
            pltpu.VMEM((NT, 2, VALUE, QT), F32),
            pltpu.VMEM((4 * NT, 8, QT), F32),
            pltpu.VMEM((Y * TOK, VALUE), BF16),
            pltpu.VMEM((2, half, VALUE), BF16),
            pltpu.VMEM((2, TOK, VALUE), BF16),
            pltpu.VMEM((2, half, VALUE), BF16),
            pltpu.VMEM((TOK, VALUE), F32),
            pltpu.VMEM((X, R, D), BF16),
            pltpu.VMEM((X, R, D), BF16),
            pltpu.VMEM((X, R, D), BF16),
            pltpu.VMEM((2, R, D // 2), BF16),
            pltpu.VMEM((2, R, D), BF16),
            pltpu.VMEM((2, R, D // 2), BF16),
            dma((5,)),
            dma((3,)), dma((3,)), dma((4,)), dma((4,)), dma((6,)), dma((6,)),
            dma((reach, 2)), dma((reach, 2)), dma((reach, 2)), dma((reach, 2)),
            dma((3,)), dma((3,)), dma((6,)), dma((6,)), dma((X,)), dma((X,)), dma((6,)), dma((6,)),
        ],
        compiler_params=pltpu.CompilerParams(
            collective_id=0, has_side_effects=True, vmem_limit_bytes=60 * 2**20
        ),
    )(
        activations, query_weight, key_weight, value_weight, out_weight, lambdas, head_gain.reshape(1, VALUE)
    )


def build(mesh, Y):
    X = mesh.shape["tp"] // 2
    Z = mesh.shape["sp"] // Y
    in_specs = (
        P(("sp", "tp"), None),
        P(None, "tp"),
        P(None, "tp"),
        P(None, "tp"),
        P("tp", None),
        P("tp"),
        P(),
    )
    out_specs = P(("sp", "tp"), None)
    return jax.shard_map(
        functools.partial(layer, X, Y, Z), mesh=mesh, in_specs=in_specs, out_specs=out_specs, check_vma=False
    )


def solution(mesh):
    return build(mesh, 4)
```

time: 388 us -> 119 us (0.31)
  waiting for transfers between devices: 124 us -> 0 us
  Pallas kernels: 0 us -> 116 us
  matrix products: 73.1 us -> 0 us
  local copies, waits for them, and re-layouts: 66.6 us -> 1.64 us
  blocking collectives: 57.2 us -> 0 us
  other arithmetic: 30.3 us -> 0 us
  loops' own time: 20.1 us -> 0 us
  between operations: 14.2 us -> 0.66 us
    all_gather x1 -> x0, waiting for transfers between devices: 124 us -> none  [in_one_piece(): lax.all_gather(both, axis, axis=dim, tiled=True)]
    pallas_call x0 -> x1, Pallas kernels: none -> 116 us  [layer(): pl.pallas_call(functools.partial(fused, X, Y, Z, TOK, D, R, QT), out_shap...]
    dot_general x58 -> x0, matrix products: 73.1 us -> none  [the longest x28 54.7 us: absorb(): jnp.einsum('hmqk,khv->hmqv', exp_weights.astype(jnp.bfloat16), value_grid...]
    all_to_all x2 -> x0, blocking collectives: 57.2 us -> none  [the longest x1 28.8 us: from_everyone(): return lax.all_to_all(copies, axis, split_axis=0, concat_axis=0, tiled=True)]
    dynamic_slice x28 -> x0, local copies, waits for them, and re-layouts: 27.2 us -> none  [one_span(): key_block = lax.dynamic_slice_in_dim(key_piece, offset, span, 0)]
    slice x31 -> x0, local copies, waits for them, and re-layouts: 27 us -> none  [the longest x28 16.6 us: one_span(): fresh.append(lax.cond(offset <= query_pos[-1], take, leave, state))]
    reduce_sum x30 -> x0, other arithmetic: 23.9 us -> none  [the longest x28 22.5 us: absorb(): denoms = denoms * factor + jnp.sum(exp_weights, axis=-1)]
    another operation x29 -> x0, loops' own time: 20.1 us -> none  [the longest x1 18.4 us: make_folder(): return lax.fori_loop(0, length // span, one_span, carry)]
  transfers between devices with their start and end apart: 1 -> 0, of which waited for: 1 -> 0; matrix products, arithmetic and copies ran while one was open for 0% -> 0% of each run, Pallas kernels for 0% -> 0%
where the time goes in v1:
time: 119 us; the launch traced here: 118 us
  Pallas kernels  116 us (97%)
  local copies, waits for them, and re-layouts  1.64 us (1%)
    pallas_call x1, Pallas kernels, layer(): pl.pallas_call(functools.partial(fused, X, Y, Z, TOK, D, R, QT), out_shap...  116 us

profile of v1, /device:TPU:240, one launch (start us, length us, event | category | flops | bytes accessed | tf_op | source)
XLA Modules:
  0.0 118.1 jit_solution(950803021575068384)
XLA Ops:
  0.7 115.8 %shard_map.73 = bf16[56,2048]{1,0:T(8,128)(2,1)} custom-call(bf16[56,2048]{1,0:T(8,128)(2,1)} %refs_0_.1, bf16[2048,256]{1,0:T(8,128)(2,1)} %refs_1_.1, bf16[2048,256]{1,0:T(8,128)(2,1)} %refs_2_.1, bf16[2048,256]{1,0:T(8,128)(2,1)} %refs_3_.1, bf16[256,2048]{1,0:T(8,128)(2,1)} %refs_4_.1, f32[1]{0:T(128)S(6)} %copy.9.refs_5_, f32[1,256]{1,0:T(1,128)} %bitcast.1), custom_call_target="tpu_custom_call" | custom-call | tf_op jit(solution)/shard_map/pallas_call | solution.py:474
  116.4 1.6 %copy.10 = bf16[56,2048]{1,0:T(8,128)(2,1)} copy(bf16[56,2048]{1,0:T(8,128)(2,1)} %shard_map.73) | data formatting | bytes 458752
